TPU v7x, 32 devices: a whole 2x2x4 slice. The times are simulated.
32 devices in a mesh: sp: 8 (over z, core), tp: 4 (over y, x).
Axes of the slice: x: 2, y: 2, z: 4, core: 2. Of those that a mesh axis runs over, the one named last changes fastest.
Arguments:
- b_gate: bfloat16 [2048, 1024], P('sp', 'tp'), may hold values from -6 to 6
- c_gate: bfloat16 [2048, 1024], P('sp', 'tp'), may hold values from -6 to 6
- h_in: bfloat16 [2048, 1024], P('sp', 'tp'), may hold values from -6 to 6
- docs: int32 [2048], replicated, may hold values from 0 to 3, never falling along the last dimension, each value on 1 to 1024 neighbouring positions
- conv_taps: bfloat16 [3, 1024], replicated, may hold values from -3 to 3
- out_weight: bfloat16 [1024, 4096], P(None, 'tp'), may hold values from -0.1875 to 0.1875
- residual_in: bfloat16 [2048, 4096], P('sp', 'tp'), may hold values from -52 to 52
- norm_gain: bfloat16 [4096], replicated, may hold values from 0.099609375 to 1.8984375
- expert_pick: int32 [2048, 2], P('sp'), may hold values from 0 to 7, as said below
- route_weight: float32 [2048, 2], P('sp'), may hold values from 0.5 to 2
- w_gate: bfloat16 [8, 4096, 2048], P('sp', None, 'tp'), may hold values from -0.09375 to 0.09375
- w_up: bfloat16 [8, 4096, 2048], P('sp', None, 'tp'), may hold values from -0.09375 to 0.09375
- w_down: bfloat16 [8, 2048, 4096], P('sp', None, 'tp'), may hold values from -0.125 to 0.125
Outputs:
- stream_out: bfloat16 [2048, 4096], P('sp', 'tp')
Inputs may be any that keep to these rules, and one draw needn't show every extreme that they name: `expert_pick`: each row names 2 different experts of one group; group g holds experts g * 2 up to the next group's first.
All inputs are finite; a program needn't handle non-finite values.
Results may differ from a plain program's by a relative error of at most 0.012.
Values may be sent and summed in bfloat16 or wider, within the bound.
A program may use at most 64 MiB of HBM per device.

v0:
```python
import jax
import jax.numpy as jnp
from jax import lax
from jax.sharding import PartitionSpec as P

TOP_K = 2


NORM_EPS = 1e-06


def passed_along(value, axis, steps):
    count = lax.axis_size(axis)
    first, last = (max(0, -steps), min(count, count - steps))
    return lax.ppermute(value, axis, [(source, source + steps) for source in range(first, last)])


def local(
    b_gate,
    c_gate,
    h_in,
    docs,
    conv_taps,
    out_weight,
    residual_in,
    norm_gain,
    expert_pick,
    route_weight,
    w_gate,
    w_up,
    w_down,
):
    tok_rows, local_chans = h_in.shape
    width = residual_in.shape[1]
    full_dim = w_gate.shape[1]
    n_sp = lax.axis_size("sp")
    sp_index = lax.axis_index("sp")
    tp_index = lax.axis_index("tp")
    first_pos = sp_index * tok_rows
    product = (c_gate.astype(jnp.float32) * h_in.astype(jnp.float32)).astype(jnp.bfloat16)
    edge = passed_along(product[tok_rows - 2 :], "sp", 1)
    extended = jnp.concatenate([edge, product], axis=0).astype(jnp.float32)
    own_docs = lax.dynamic_slice_in_dim(docs, first_pos, tok_rows)
    padded_docs = jnp.concatenate([jnp.full((2,), -1, jnp.int32), docs], axis=0)
    near_docs = lax.dynamic_slice_in_dim(padded_docs, first_pos, tok_rows + 2)
    tap_weights = lax.dynamic_slice_in_dim(
        conv_taps, tp_index * local_chans, local_chans, 1
    ).astype(jnp.float32)
    conv_sum = tap_weights[0][None, :] * extended[2:]
    for step_back in (1, 2):
        same_doc = (near_docs[2 - step_back : 2 - step_back + tok_rows] == own_docs).astype(
            jnp.float32
        )[:, None]
        conv_sum = (
            conv_sum
            + tap_weights[step_back][None, :]
            * extended[2 - step_back : 2 - step_back + tok_rows]
            * same_doc
        )
    conv_out = (b_gate.astype(jnp.float32) * conv_sum).astype(jnp.bfloat16)
    projected = jnp.dot(
        lax.all_gather(conv_out, "tp", axis=1, tiled=True),
        out_weight,
        preferred_element_type=jnp.float32,
    )
    stream = (residual_in.astype(jnp.float32) + projected).astype(jnp.bfloat16)
    stream_f = stream.astype(jnp.float32)
    capacity = 5 * tok_rows // (2 * n_sp)
    assign_flat = expert_pick.reshape(-1)
    onehot = (assign_flat[:, None] == jnp.arange(n_sp, dtype=jnp.int32)[None, :]).astype(jnp.int32)
    slot_pos = jnp.sum((jnp.cumsum(onehot, axis=0) - onehot) * onehot, axis=1)
    kept_mask = slot_pos < capacity
    target = jnp.where(
        kept_mask, assign_flat * capacity + jnp.minimum(slot_pos, capacity - 1), n_sp * capacity
    )
    table = (
        jnp.full((n_sp * capacity + 1,), -1, jnp.int32)
        .at[target]
        .set(jnp.arange(assign_flat.shape[0], dtype=jnp.int32))[:-1]
    )
    filled = table >= 0
    source_rows = jnp.maximum(table, 0) // TOP_K
    gate_local = w_gate[0]
    up_local = w_up[0]
    slot_rows = n_sp * capacity
    squares = lax.psum(jnp.sum(stream_f * stream_f, axis=1), "tp")
    inverse = lax.rsqrt(squares / full_dim + NORM_EPS)[:, None]
    gain_cols = lax.dynamic_slice_in_dim(norm_gain, tp_index * width, width).astype(jnp.float32)
    normed = (stream_f * inverse * gain_cols[None, :]).astype(jnp.bfloat16)
    outgoing = jnp.where(filled[:, None], normed[source_rows], jnp.zeros((), normed.dtype)).reshape(
        n_sp, capacity, width
    )
    received = lax.all_to_all(outgoing, "sp", split_axis=0, concat_axis=0, tiled=True)
    shard_piece = lax.all_gather(received, "tp", axis=2, tiled=True)
    flat_piece = shard_piece.reshape(slot_rows, shard_piece.shape[2])
    gate_pre = jnp.dot(flat_piece, gate_local, preferred_element_type=jnp.float32)
    up_pre = jnp.dot(flat_piece, up_local, preferred_element_type=jnp.float32)
    hidden = (jax.nn.silu(gate_pre) * up_pre).astype(jnp.bfloat16)
    down_local = w_down[0]
    result = jnp.dot(
        lax.all_gather(hidden, "tp", axis=1, tiled=True),
        down_local,
        preferred_element_type=jnp.float32,
    ).astype(jnp.bfloat16)
    returned = lax.all_to_all(
        result.reshape(n_sp, capacity, width), "sp", split_axis=0, concat_axis=0, tiled=True
    ).reshape(n_sp * capacity, width)
    picked = jnp.where(
        kept_mask[:, None],
        returned[jnp.minimum(target, n_sp * capacity - 1)].astype(jnp.float32),
        0.0,
    )
    weighted = picked * route_weight.reshape(-1)[:, None]
    feed_out = jnp.sum(weighted.reshape(tok_rows, TOP_K, width), axis=1)
    return (stream_f + feed_out).astype(jnp.bfloat16)


def solution(mesh):
    return jax.shard_map(
        local,
        mesh=mesh,
        in_specs=(
            P("sp", "tp"),
            P("sp", "tp"),
            P("sp", "tp"),
            P(),
            P(),
            P(None, "tp"),
            P("sp", "tp"),
            P(),
            P("sp", None),
            P("sp", None),
            P("sp", None, "tp"),
            P("sp", None, "tp"),
            P("sp", None, "tp"),
        ),
        out_specs=P("sp", "tp"),
        check_vma=False,
    )
```

profile of v0, /device:TPU:0, one launch (start us, length us, event | category | flops | bytes accessed | tf_op | source)
XLA Modules:
  0.0 260.3 jit_solution(9669423015625379213)
XLA Ops:
  6.5 1.1 multiply_convert_fusion
  7.7 2.4 collective-permute-start
  10.1 0.8 copy.15
  11.2 1.1 reduce-window.6
  13.8 2.4 scatter_custom_fusion
  17.0 0.8 pad_dynamic-slice_fusion
  19.3 1.1 fusion.23
  20.4 16.3 %all_gather.9 = bf16[256,1024]{1,0:T(8,128)(2,1)S(1)} all-gather(bf16[256,256]{1,0:T(8,128)(2,1)S(1)} %fusion.23), channel_id=1, replica_groups=mesh['sp'=8,'tp'=4] {'tp'}, dimensions={1}, use_global_device_ids=true | all-gather | bytes 655360 | tf_op jit(solution)/shard_map/all_gather | solution.py:62
  36.7 0.8 fusion.16
  37.5 9.0 %psum.7 = f32[256]{0:T(256)S(1)} all-reduce(f32[256]{0:T(256)S(1)} %get-tuple-element.12), channel_id=1, replica_groups=mesh['sp'=8,'tp'=4] {'tp'}, use_global_device_ids=true, to_apply=%region_5.6 | all-reduce | flops 256 | bytes 2048 | tf_op jit(solution)/shard_map/psum | solution.py:86
  46.7 3.5 %gather_fusion = bf16[640,1024]{1,0:T(8,128)(2,1)} fusion(bf16[256,1024]{1,0:T(8,128)(2,1)S(1)} %fusion.18, s32[1024]{0:T(1024)S(1)} %pad_clamp_fusion.1), kind=kCustom, calls=%fused_computation | custom fusion | bytes 2624000 | tf_op jit(solution)/shard_map/gather | solution.py:90
  50.1 1.5 broadcast_select_fusion
  51.6 36.2 %all_to_all.10 = bf16[8,80,1024]{2,1,0:T(8,128)(2,1)} all-to-all(bf16[8,80,1024]{2,1,0:T(8,128)(2,1)S(1)} %broadcast_select_fusion), channel_id=1, replica_groups=mesh['sp'=8,'tp'=4] {'sp'}, dimensions={0} | all-to-all | bytes 2621440 | tf_op jit(solution)/shard_map/all_to_all | solution.py:93
  87.9 59.4 %all-gather.3.cloned.1.call-done = bf16[8,80,4096]{2,1,0:T(8,128)(2,1)} async-done(((bf16[8,80,1024]{2,1,0:T(8,128)(2,1)}), bf16[8,80,4096]{2,1,0:T(8,128)(2,1)}) %all-gather.3.cloned.1.call-update) | async-done | bytes 5242896 | tf_op jit(solution)/shard_map/all_gather | solution.py:94
  147.2 6.2 %fusion.4 = f32[640,512]{1,0:T(8,128)S(1)} fusion(bf16[640,4096]{1,0:T(8,128)(2,1)} %bitcast.47, bf16[1,4096,512]{2,1,0:T(8,128)(2,1)} %param.23), kind=kOutput, calls=%fused_computation.7 | convolution fusion | flops 2684354560 | bytes 10747904 | tf_op jit(solution)/shard_map/dot_general | solution.py:96
  153.7 3.8 %fusion.12 = bf16[640,512]{1,0:T(8,128)(2,1)} fusion(bf16[640,4096]{1,0:T(8,128)(2,1)S(1)} %bitcast.48, bf16[1,4096,512]{2,1,0:T(8,128)(2,1)S(1)} %copy-done.6, f32[640,512]{1,0:T(8,128)S(1)} %fusion.4), kind=kOutput, calls=%fused_computation.16 | convolution fusion | flops 2686320640 | bytes 11403264 | tf_op jit(solution)/shard_map/dot_general | solution.py:97
  157.6 39.5 %all-gather.5.cloned.1.call-done = bf16[640,2048]{1,0:T(8,128)(2,1)} async-done(((bf16[640,512]{1,0:T(8,128)(2,1)}), bf16[640,2048]{1,0:T(8,128)(2,1)}) %all-gather.5.cloned.1.call-update) | async-done | bytes 2621456 | tf_op jit(solution)/shard_map/all_gather | solution.py:101
  197.1 6.9 %fusion.6 = bf16[640,1024]{1,0:T(8,128)(2,1)} fusion(bf16[640,2048]{1,0:T(8,128)(2,1)} %all-gather.5.cloned.1.call-done, bf16[1,2048,1024]{2,1,0:T(8,128)(2,1)} %param.25), kind=kOutput, calls=%fused_computation.10 | convolution fusion | flops 2685009920 | bytes 8126464 | tf_op jit(solution)/shard_map/dot_general | solution.py:100
  204.1 4.7 %all-to-all-start.1 = ((bf16[8,80,1024]{2,1,0:T(8,128)(2,1)}), bf16[8,80,1024]{2,1,0:T(8,128)(2,1)S(1)}, u32[]{:S(2)}, u32[]{:S(2)}) async-start(bf16[8,80,1024]{2,1,0:T(8,128)(2,1)} %bitcast.40), calls=%async_computation.1 | async-start | bytes 2621440 | tf_op jit(solution)/shard_map/all_to_all | solution.py:105
  209.7 31.2 %all-to-all-done.1 = bf16[8,80,1024]{2,1,0:T(8,128)(2,1)S(1)} async-done(((bf16[8,80,1024]{2,1,0:T(8,128)(2,1)}), bf16[8,80,1024]{2,1,0:T(8,128)(2,1)S(1)}, u32[]{:S(2)}, u32[]{:S(2)}) %all-to-all-start.1) | async-done | bytes 1310752 | tf_op jit(solution)/shard_map/all_to_all | solution.py:105
  241.0 2.8 %gather_fusion.1 = bf16[512,1024]{1,0:T(8,128)(2,1)} fusion(bf16[640,1024]{1,0:T(8,128)(2,1)S(1)} %bitcast.38, s32[1024]{0:T(1024)S(1)} %pad_clamp_fusion), kind=kCustom, calls=%fused_computation.1 | custom fusion | bytes 2099200 | tf_op jit(solution)/shard_map/gather | solution.py:110
  243.8 3.4 %reshape.127 = f32[256,2,1024]{2,1,0:T(2,128)} reshape(bf16[512,1024]{1,0:T(8,128)(2,1)} %gather_fusion.1) | data formatting | bytes 3145728 | tf_op jit(solution)/shard_map/convert_element_type | solution.py:110
  247.2 5.4 %multiply_reduce_fusion = f32[256,1024]{1,0:T(8,128)S(1)} fusion(f32[256,2,1024]{2,1,0:T(2,128)} %reshape.127, pred[256,2]{1,0:T(8,128)(4,1)S(1)} %copy-done.3, f32[256,2]{1,0:T(8,128)S(1)} %copy.18), kind=kLoop, calls=%fused_computation.9 | loop fusion | flops 1310720 | bytes 3148288 | tf_op jit(solution)/shard_map/reduce_sum | solution.py:114
  252.5 0.9 fusion.19
  (50 shorter events, 5.4 us)
Async XLA Ops:
  6.5 30.1 %copy-start = (bf16[1024,1024]{1,0:T(8,128)(2,1)S(1)}, bf16[1024,1024]{1,0:T(8,128)(2,1)}, u32[]{:S(2)}) copy-start(bf16[1024,1024]{1,0:T(8,128)(2,1)} %param.18) | copy-start | bytes 6291460
  6.5 30.1 %copy-start.7 = (bf16[256,1024]{1,0:T(8,128)(2,1)S(1)}, bf16[256,1024]{1,0:T(8,128)(2,1)}, u32[]{:S(2)}) copy-start(bf16[256,1024]{1,0:T(8,128)(2,1)} %param.19) | copy-start | bytes 1572868
  6.5 140.7 %all-gather.3.cloned.1.call-start = ((), (), s32[]{:S(2)}) async-start(), calls=%async_computation.2 | async-start | bytes 6553600 | tf_op jit(solution)/shard_map/all_gather | solution.py:94
  7.7 11.6 %collective-permute-start = (bf16[2,256]{1,0:T(2,128)(2,1)S(1)}, bf16[2,256]{1,0:T(2,128)(2,1)S(1)}, u32[]{:S(2)}, u32[]{:S(2)}) collective-permute-start(bf16[2,256]{1,0:T(2,128)(2,1)S(1)} %slice.53), channel_id=1, source_target_pairs={{0,4},{4,8},{8,12},{12,16},{16,20},{20,24},{24,28},{1,5},{5,9},{9,... | collective-permute-start | bytes 3080 | tf_op jit(solution)/shard_map/ppermute | solution.py:15
  37.5 12.7 %copy-start.1 = (bf16[256,1024]{1,0:T(8,128)(2,1)}, bf16[256,1024]{1,0:T(8,128)(2,1)S(1)}, u32[]{:S(2)}) copy-start(bf16[256,1024]{1,0:T(8,128)(2,1)S(1)} %get-tuple-element.13) | copy-start | bytes 1572868
  87.8 109.3 %all-gather.5.cloned.1.call-start = ((), (), s32[]{:S(2)}) async-start(), calls=%async_computation.3 | async-start | bytes 3276800 | tf_op jit(solution)/shard_map/all_gather | solution.py:101
  147.2 6.2 %copy-start.5 = (bf16[8,80,4096]{2,1,0:T(8,128)(2,1)S(1)}, bf16[8,80,4096]{2,1,0:T(8,128)(2,1)}, u32[]{:S(2)}) copy-start(bf16[8,80,4096]{2,1,0:T(8,128)(2,1)} %all-gather.3.cloned.1.call-done) | copy-start | bytes 15728644
  147.2 6.5 %copy-start.6 = (bf16[1,4096,512]{2,1,0:T(8,128)(2,1)S(1)}, bf16[1,4096,512]{2,1,0:T(8,128)(2,1)}, u32[]{:S(2)}) copy-start(bf16[1,4096,512]{2,1,0:T(8,128)(2,1)} %param.24) | copy-start | bytes 12582916
  204.1 5.5 %copy-start.4 = (f32[256,2]{0,1:T(2,128)S(1)}, f32[256,2]{0,1:T(2,128)}, u32[]{:S(2)}) copy-start(f32[256,2]{0,1:T(2,128)} %param.22) | copy-start | bytes 6148
  204.1 36.9 %all-to-all-start.1 = ((bf16[8,80,1024]{2,1,0:T(8,128)(2,1)}), bf16[8,80,1024]{2,1,0:T(8,128)(2,1)S(1)}, u32[]{:S(2)}, u32[]{:S(2)}) async-start(bf16[8,80,1024]{2,1,0:T(8,128)(2,1)} %bitcast.40), calls=%async_computation.1 | async-start | bytes 2621440 | tf_op jit(solution)/shard_map/all_to_all | solution.py:105
  243.8 3.4 %copy-start.3 = (pred[256,2]{1,0:T(8,128)(4,1)S(1)}, pred[256,2]{1,0:T(8,128)(4,1)}, u32[]{:S(2)}) copy-start(pred[256,2]{1,0:T(8,128)(4,1)} %lt.59) | copy-start | bytes 1540
  247.2 5.4 %copy-start.2 = (bf16[256,1024]{1,0:T(8,128)(2,1)S(1)}, bf16[256,1024]{1,0:T(8,128)(2,1)}, u32[]{:S(2)}) copy-start(bf16[256,1024]{1,0:T(8,128)(2,1)} %copy-done.1) | copy-start | bytes 1572868
Sparse Core Ops, SparseCore 0:
  87.9 59.2 all-gather.2
  157.7 39.3 all-gather.4
where the time goes:
time: 261 us; the launch traced here: 260 us
  waiting for transfers between devices  130 us (50%)
  blocking collectives  61.4 us (24%)
  matrix products  17.8 us (7%)
  local copies, waits for them, and re-layouts  15.8 us (6%)
  other arithmetic  14.4 us (6%)
  between operations  13.6 us (5%)
  starting transfers between devices  7.18 us (3%)
    all_gather x1, waiting for transfers between devices, local(): shard_piece = lax.all_gather(received, 'tp', axis=2, tiled=True)  59.4 us
    all_gather x1, waiting for transfers between devices, local(): lax.all_gather(hidden, 'tp', axis=1, tiled=True)  39.5 us
    all_to_all x1, blocking collectives, local(): lax.all_to_all(outgoing, 'sp', split_axis=0, concat_axis=0, tiled=True)  36.2 us
    all_to_all x1, waiting for transfers between devices, local(): lax.all_to_all(result.reshape(n_sp, capacity, width), 'sp', split_axis=0,...  31.2 us
    all_gather x1, blocking collectives, local(): lax.all_gather(conv_out, 'tp', axis=1, tiled=True)  16.3 us
    psum x1, blocking collectives, local(): squares = lax.psum(jnp.sum(stream_f * stream_f, axis=1), 'tp')  8.96 us
    dot_general x1, matrix products, local(): jnp.dot(lax.all_gather(hidden, 'tp', axis=1, tiled=True), down_local, pre...  6.94 us
    dot_general x1, matrix products, local(): jnp.dot(flat_piece, gate_local, preferred_element_type=jnp.float32)  6.17 us
  transfers between devices with their start and end apart: 4, of which 3 were waited for; matrix products, arithmetic and copies ran while one was open for 4% of the time, Pallas kernels for 0%

commit v1 on v0

--- a/solution.py
+++ b/solution.py
@@ -1,9 +1,15 @@
+import functools
+
 import jax
 import jax.numpy as jnp
 from jax import lax
+from jax.experimental import pallas as pl
+from jax.experimental.pallas import tpu as pltpu
 from jax.sharding import PartitionSpec as P
 
 TOP_K = 2
+GROUPS = 4
+MESH = pl.DeviceIdType.MESH
 
 
 NORM_EPS = 1e-06
@@ -15,7 +21,7 @@
     return lax.ppermute(value, axis, [(source, source + steps) for source in range(first, last)])
 
 
-def local(
+def general(
     b_gate,
     c_gate,
     h_in,
@@ -115,9 +121,423 @@
     return (stream_f + feed_out).astype(jnp.bfloat16)
 
 
+def flipped(index, mask):
+    bit = 1
+    while bit <= mask:
+        if mask & bit:
+            index = index + bit * (1 - 2 * ((index // bit) % 2))
+        bit *= 2
+    return index
+
+
+def fused_kernel(
+    n_chips,
+    capacity,
+    b_ref,
+    c_ref,
+    h_ref,
+    cols_ref,
+    taps_ref,
+    resid_ref,
+    gain_ref,
+    ow_hbm,
+    wg_hbm,
+    wu_hbm,
+    wd_hbm,
+    out_ref,
+    ow,
+    wg,
+    wu,
+    wd,
+    ext,
+    cv,
+    stream,
+    acc,
+    pt,
+    rows_out,
+    wts_out,
+    rows,
+    wts,
+    normed,
+    hid,
+    e_own,
+    e_send,
+    e_recv,
+    feed_out,
+    back,
+    local_sems,
+    send_sems,
+    recv_sems,
+):
+    tok_rows, chans = h_ref.shape
+    width = resid_ref.shape[1]
+    full = gain_ref.shape[1]
+    hid_cols = wg.shape[1]
+    sp = lax.axis_index("sp")
+    tp = lax.axis_index("tp")
+    chip = sp // 2
+    core = sp % 2
+    tp_x = (tp // 2) * 2 + (1 - tp % 2)
+    tp_y = (1 - tp // 2) * 2 + tp % 2
+    tp_d = (1 - tp // 2) * 2 + (1 - tp % 2)
+    dev_x = (sp, tp_x)
+    dev_y = (sp, tp_y)
+    dev_s = (chip * 2 + (1 - core), tp)
+    ks = list(range(n_chips))
+    dev_z = [(flipped(chip, k) * 2 + core, tp) for k in ks]
+
+    loads = []
+    for i, (s, d) in enumerate(((ow_hbm, ow), (wg_hbm.at[0], wg), (wu_hbm.at[0], wu), (wd_hbm.at[0], wd))):
+        cp = pltpu.make_async_copy(s, d, local_sems.at[i])
+        cp.start()
+        loads.append(cp)
+
+    count = [0]
+    sent = []
+
+    def remote(s, d, dev):
+        i = count[0]
+        count[0] += 1
+        return pltpu.make_async_remote_copy(
+            src_ref=s, dst_ref=d, send_sem=send_sems.at[i], recv_sem=recv_sems.at[i],
+            device_id=dev, device_id_type=MESH,
+        )
+
+    def go(s, d, dev):
+        cp = remote(s, d, dev)
+        cp.start()
+        sent.append(cp)
+        return cp
+
+    def cols(index, size):
+        return pl.ds(pl.multiple_of(index * size, 128), size)
+
+    barrier = pltpu.get_barrier_semaphore()
+    peers = [dev_x, dev_y, dev_s] + dev_z[1:]
+    for dev in peers:
+        pl.semaphore_signal(barrier, inc=1, device_id=dev, device_id_type=MESH)
+    other = jnp.where(core == 0, sp - 1, sp + 1)
+    has_other = jnp.where(core == 0, chip > 0, chip < n_chips - 1)
+
+    @pl.when(has_other)
+    def _():
+        pl.semaphore_signal(barrier, inc=1, device_id=(other, tp), device_id_type=MESH)
+
+    product = (c_ref[...].astype(jnp.float32) * h_ref[...].astype(jnp.float32)).astype(jnp.bfloat16)
+    ext[8:, :] = product.astype(jnp.float32)
+    pl.semaphore_wait(barrier, len(peers) + has_other.astype(jnp.int32))
+
+    edge = remote(ext.at[pl.ds(tok_rows, 8)], ext.at[pl.ds(0, 8)], (sp + 1, tp))
+
+    @pl.when(sp < 2 * n_chips - 1)
+    def _():
+        edge.start()
+
+    lane = lax.broadcasted_iota(jnp.int32, (tok_rows, 128), 1)
+    lane_f = lane.astype(jnp.float32)
+    group = cols_ref[:, 2:3]
+    onehot = (group == lane_f).astype(jnp.float32)
+    earlier = (
+        lax.broadcasted_iota(jnp.int32, (tok_rows, tok_rows), 1)
+        < lax.broadcasted_iota(jnp.int32, (tok_rows, tok_rows), 0)
+    ).astype(jnp.float32).astype(jnp.bfloat16)
+    before = jnp.dot(earlier, onehot.astype(jnp.bfloat16), preferred_element_type=jnp.float32)
+    slot = jnp.sum(before * onehot, axis=1, keepdims=True)
+    for k in ks:
+        here = flipped(chip, k).astype(jnp.float32)
+        hit = jnp.where((group == here) & (slot == lane_f) & (lane < capacity), 1.0, 0.0)
+        pt[k] = hit.astype(jnp.bfloat16)
+    parts = jnp.zeros((tok_rows, 128), jnp.float32)
+    for j in range(2):
+        w = cols_ref[:, 3 + j : 4 + j]
+        for i in range(3):
+            piece = w.astype(jnp.bfloat16).astype(jnp.float32)
+            parts = jnp.where(lane == 3 * j + i, piece, parts)
+            w = w - piece
+    parts = parts.astype(jnp.bfloat16)
+    for k in ks:
+        got = lax.dot_general(
+            pt[k], parts, (((0,), (0,)), ((), ())), preferred_element_type=jnp.float32
+        )
+        wts_out[k] = got[:capacity].astype(jnp.bfloat16)
+    wts[0] = wts_out[0]
+
+    @pl.when(sp > 0)
+    def _():
+        edge.wait_recv()
+
+    @pl.when(sp == 0)
+    def _():
+        ext[0:8, :] = jnp.zeros((8, chans), jnp.float32)
+
+    taps = taps_ref[:, cols(tp, chans)].astype(jnp.float32)
+    conv = taps[0:1, :] * ext[8 : 8 + tok_rows, :]
+    for lag in (1, 2):
+        conv = conv + taps[lag : lag + 1, :] * ext[8 - lag : 8 - lag + tok_rows, :] * cols_ref[:, lag - 1 : lag]
+    conv = (b_ref[...].astype(jnp.float32) * conv).astype(jnp.bfloat16)
+    cv[:, cols(tp, chans)] = conv
+
+    def spread(buf, size, own_sends):
+        mine = buf.at[:, cols(tp, size)]
+        own_sends.append(go(mine, mine, dev_x))
+        own_sends.append(go(mine, mine, dev_y))
+
+    def relay(buf, size, sends):
+        half = size // 2
+        sends[1].wait_recv()
+        part = buf.at[:, cols(tp_y * 2, half)]
+        sends.append(go(part, part, dev_x))
+        sends[0].wait_recv()
+        part = buf.at[:, cols(tp_x * 2 + 1, half)]
+        sends.append(go(part, part, dev_y))
+
+    conv_sends = []
+    spread(cv, chans, conv_sends)
+
+    def proj(index):
+        rows_ = pl.ds(pl.multiple_of(index * chans, 128), chans)
+        return jnp.dot(cv[:, cols(index, chans)], ow[rows_, :], preferred_element_type=jnp.float32)
+
+    loads[0].wait()
+    acc[...] = resid_ref[...].astype(jnp.float32) + proj(tp)
+    relay(cv, chans, conv_sends)
+    acc[...] += proj(tp_x)
+    acc[...] += proj(tp_y)
+    conv_sends[2].wait_recv()
+    conv_sends[3].wait_recv()
+    stream[...] = (acc[...] + proj(tp_d)).astype(jnp.bfloat16)
+
+    z_rows, z_wts = [None] * n_chips, [None] * n_chips
+    mine = cols(tp, width)
+    for k in [0] + ks[1:]:
+        got = lax.dot_general(
+            pt[k], stream[...], (((0,), (0,)), ((), ())), preferred_element_type=jnp.float32
+        )[:capacity].astype(jnp.bfloat16)
+        if k == 0:
+            rows[0, 0, :, mine] = got
+        else:
+            rows_out[k] = got
+            z_rows[k] = go(rows_out.at[k], rows.at[k, 0, :, mine], dev_z[k])
+        if k == 0:
+            row_sends = [[] for _ in ks]
+            sis = [[] for _ in ks]
+            first = True
+            spread(rows.at[0, 0], width, row_sends[0])
+            sis[0].append(go(rows.at[0, 0, :, mine], rows.at[0, 1, :, mine], dev_s))
+    for k in ks[1:]:
+        z_wts[k] = go(wts_out.at[k], wts.at[k], dev_z[k])
+
+    def share(k, index, size):
+        at = cols(index, size)
+        sis[k].append(go(rows.at[k, 0, :, at], rows.at[k, 1, :, at], dev_s))
+
+    def stage(k):
+        if k > 0:
+            z_rows[k].wait_recv()
+            spread(rows.at[k, 0], width, row_sends[k])
+            share(k, tp, width)
+
+    def forward(k):
+        relay(rows.at[k, 0], width, row_sends[k])
+        share(k, tp_x, width)
+        share(k, tp_y, width)
+
+    def finish(k):
+        row_sends[k][2].wait_recv()
+        share(k, tp_d * 2, width // 2)
+        row_sends[k][3].wait_recv()
+        share(k, tp_d * 2 + 1, width // 2)
+
+    hid_sends = [[] for _ in ks]
+
+    def expand(k):
+        for cp in sis[k]:
+            cp.wait_recv()
+        for p in range(2):
+            def norm(r, carry, p=p):
+                at = pl.ds(pl.multiple_of(r * 16, 16), 16)
+                x = rows[k, p, at, :].astype(jnp.float32)
+                ms = jnp.sum(x * x, axis=1, keepdims=True) / full
+                inv = lax.rsqrt(ms + NORM_EPS)
+                y = (x * inv * gain_ref[...]).astype(jnp.bfloat16)
+                normed[pl.ds(pl.multiple_of(p * capacity + r * 16, 16), 16), :] = y
+                return carry
+            lax.fori_loop(0, capacity // 16, norm, 0)
+        if k == 0:
+            loads[1].wait()
+            loads[2].wait()
+
+        def tile(n, carry):
+            at = pl.ds(pl.multiple_of(n * 256, 256), 256)
+            x = normed[...]
+            g = jnp.dot(x, wg[:, at], preferred_element_type=jnp.float32)
+            u = jnp.dot(x, wu[:, at], preferred_element_type=jnp.float32)
+            h = (g / (1.0 + jnp.exp(-g)) * u).astype(jnp.bfloat16)
+            hid[k, :, pl.ds(pl.multiple_of(tp * hid_cols + n * 256, 256), 256)] = h
+            return carry
+
+        lax.fori_loop(0, hid_cols // 256, tile, 0)
+        spread(hid.at[k], hid_cols, hid_sends[k])
+
+    def hid_forward(k):
+        relay(hid.at[k], hid_cols, hid_sends[k])
+
+    e_sends = [None] * n_chips
+    z_back = [None] * n_chips
+
+    def down(k):
+        hid_sends[k][2].wait_recv()
+        hid_sends[k][3].wait_recv()
+        if k == 0:
+            loads[3].wait()
+
+        def tile(n, carry):
+            at = pl.ds(pl.multiple_of(n * 256, 256), 256)
+            e = jnp.dot(hid[k], wd[:, at], preferred_element_type=jnp.float32).astype(jnp.bfloat16)
+            e_own[k, :, at] = e[:capacity]
+            e_send[k, :, at] = e[capacity:]
+            return carry
+
+        lax.fori_loop(0, width // 256, tile, 0)
+        e_sends[k] = go(e_send.at[k], e_recv.at[k], dev_s)
+
+    def combine(k):
+        if k > 0:
+            z_wts[k].wait_recv()
+        w = wts[k].astype(jnp.float32)
+        w_lane = lax.broadcasted_iota(jnp.int32, w.shape, 1)
+        w_even = jnp.sum(jnp.where(w_lane < 3, w, 0.0), axis=1, keepdims=True)
+        w_odd = jnp.sum(jnp.where((w_lane >= 3) & (w_lane < 6), w, 0.0), axis=1, keepdims=True)
+        pick = core.astype(jnp.float32)
+        w_mine = w_even * (1.0 - pick) + w_odd * pick
+        w_other = w_odd * (1.0 - pick) + w_even * pick
+        e_sends[k].wait_recv()
+        f = (e_own[k].astype(jnp.float32) * w_mine + e_recv[k].astype(jnp.float32) * w_other).astype(jnp.bfloat16)
+        if k == 0:
+            back[0, 0:capacity, :] = f
+        else:
+            feed_out[k] = f
+            z_back[k] = go(feed_out.at[k], back.at[k, pl.ds(0, capacity), :], dev_z[k])
+
+    for k in ks:
+        back[k, capacity:, :] = jnp.zeros((128 - capacity, width), jnp.bfloat16)
+
+    last = n_chips - 1
+    plan = sorted(
+        [(3 * k, 0, stage, k) for k in ks]
+        + [(3 * k + 4, 1, forward, k) for k in ks]
+        + [(3 * k + 7, 2, finish, k) for k in ks]
+        + [(3 * k + 9, 3, expand, k) for k in ks]
+        + [(3 * k + 13, 4, hid_forward, k) for k in ks]
+        + [(3 * k + 16, 5, down, k) for k in ks]
+        + [(3 * k + 18, 6, combine, k) for k in ks],
+        key=lambda item: item[:2],
+    )
+    for _, _, step, k in plan:
+        step(k)
+
+    acc[...] = stream[...].astype(jnp.float32)
+    for k in ks:
+        if k > 0:
+            z_back[k].wait_recv()
+        acc[...] += jnp.dot(pt[k], back[k], preferred_element_type=jnp.float32)
+    out_ref[...] = acc[...].astype(jnp.bfloat16)
+
+    for cp in sent:
+        cp.wait_send()
+
+    @pl.when(sp < 2 * n_chips - 1)
+    def _():
+        edge.wait_send()
+
+
+def fused(
+    b_gate,
+    c_gate,
+    h_in,
+    docs,
+    conv_taps,
+    out_weight,
+    residual_in,
+    norm_gain,
+    expert_pick,
+    route_weight,
+    w_gate,
+    w_up,
+    w_down,
+):
+    tok_rows, chans = h_in.shape
+    width = residual_in.shape[1]
+    full = w_gate.shape[1]
+    hid_cols = w_gate.shape[2]
+    hid_full = w_down.shape[1]
+    n_sp = lax.axis_size("sp")
+    n_chips = n_sp // 2
+    capacity = 5 * tok_rows // (2 * n_sp)
+    first_pos = lax.axis_index("sp") * tok_rows
+    padded_docs = jnp.concatenate([jnp.full((2,), -1, jnp.int32), docs], axis=0)
+    near = lax.dynamic_slice_in_dim(padded_docs, first_pos, tok_rows + 2)
+    own = near[2:]
+    even = expert_pick[:, 0] % 2 == 0
+    side = jnp.stack(
+        [
+            (near[1:-1] == own).astype(jnp.float32),
+            (near[:-2] == own).astype(jnp.float32),
+            (expert_pick[:, 0] // 2).astype(jnp.float32),
+            jnp.where(even, route_weight[:, 0], route_weight[:, 1]),
+            jnp.where(even, route_weight[:, 1], route_weight[:, 0]),
+        ],
+        axis=1,
+    )
+    gain = norm_gain.astype(jnp.float32)[None, :]
+    n_copies = 5 + 2 * (n_chips - 1) + 14 * n_chips + n_chips - 1
+    vmem = pl.BlockSpec(memory_space=pltpu.VMEM)
+    hbm = pl.BlockSpec(memory_space=pl.ANY)
+    bf16 = jnp.bfloat16
+    return pl.pallas_call(
+        functools.partial(fused_kernel, n_chips, capacity),
+        out_shape=jax.ShapeDtypeStruct((tok_rows, width), bf16),
+        in_specs=[vmem] * 7 + [hbm] * 4,
+        out_specs=vmem,
+        scratch_shapes=[
+            pltpu.VMEM(out_weight.shape, bf16),
+            pltpu.VMEM(w_gate.shape[1:], bf16),
+            pltpu.VMEM(w_up.shape[1:], bf16),
+            pltpu.VMEM(w_down.shape[1:], bf16),
+            pltpu.VMEM((tok_rows + 8, chans), jnp.float32),
+            pltpu.VMEM((tok_rows, out_weight.shape[0]), bf16),
+            pltpu.VMEM((tok_rows, width), bf16),
+            pltpu.VMEM((tok_rows, width), jnp.float32),
+            pltpu.VMEM((n_chips, tok_rows, 128), bf16),
+            pltpu.VMEM((n_chips, capacity, width), bf16),
+            pltpu.VMEM((n_chips, capacity, 128), bf16),
+            pltpu.VMEM((n_chips, 2, capacity, full), bf16),
+            pltpu.VMEM((n_chips, capacity, 128), bf16),
+            pltpu.VMEM((2 * capacity, full), bf16),
+            pltpu.VMEM((n_chips, 2 * capacity, hid_full), bf16),
+            pltpu.VMEM((n_chips, capacity, width), bf16),
+            pltpu.VMEM((n_chips, capacity, width), bf16),
+            pltpu.VMEM((n_chips, capacity, width), bf16),
+            pltpu.VMEM((n_chips, capacity, width), bf16),
+            pltpu.VMEM((n_chips, 128, width), bf16),
+            pltpu.SemaphoreType.DMA((4,)),
+            pltpu.SemaphoreType.DMA((n_copies,)),
+            pltpu.SemaphoreType.DMA((n_copies,)),
+        ],
+        compiler_params=pltpu.CompilerParams(
+            collective_id=0, has_side_effects=True, vmem_limit_bytes=56 * 1024 * 1024
+        ),
+    )(b_gate, c_gate, h_in, side, conv_taps, residual_in, gain, out_weight, w_gate, w_up, w_down)
+
+
+def pairs_fit(mesh):
+    n_sp, n_tp = mesh.shape["sp"], mesh.shape["tp"]
+    return n_sp == GROUPS * TOP_K and TOP_K == 2 and n_tp == 4
+
+
 def solution(mesh):
     return jax.shard_map(
-        local,
+        fused if pairs_fit(mesh) else general,
         mesh=mesh,
         in_specs=(
             P("sp", "tp"),

time: 261 us -> 87.9 us (0.34)
  waiting for transfers between devices: 130 us -> 0 us
  Pallas kernels: 0 us -> 80 us
  blocking collectives: 61.4 us -> 0 us
  matrix products: 17.8 us -> 0 us
  between operations: 13.6 us -> 0.02 us
  local copies, waits for them, and re-layouts: 15.8 us -> 3.46 us
  other arithmetic: 14.4 us -> 3.6 us
  starting transfers between devices: 7.18 us -> 0 us
    all_gather x2 -> x0, waiting for transfers between devices: 98.9 us -> none  [the longest x1 59.4 us: local(): shard_piece = lax.all_gather(received, 'tp', axis=2, tiled=True)]
    pallas_call x0 -> x1, Pallas kernels: none -> 80 us  [fused(): pl.pallas_call(functools.partial(fused_kernel, n_chips, capacity), out_sh...]
    all_to_all x1 -> x0, blocking collectives: 36.2 us -> none  [local(): lax.all_to_all(outgoing, 'sp', split_axis=0, concat_axis=0, tiled=True)]
    all_to_all x1 -> x0, waiting for transfers between devices: 31.2 us -> none  [local(): lax.all_to_all(result.reshape(n_sp, capacity, width), 'sp', split_axis=0,...]
    dot_general x4 -> x0, matrix products: 17.8 us -> none  [the longest x1 6.94 us: local(): jnp.dot(lax.all_gather(hidden, 'tp', axis=1, tiled=True), down_local, pre...]
    all_gather x1 -> x0, blocking collectives: 16.3 us -> none  [local(): lax.all_gather(conv_out, 'tp', axis=1, tiled=True)]
    psum x1 -> x0, blocking collectives: 8.96 us -> none  [local(): squares = lax.psum(jnp.sum(stream_f * stream_f, axis=1), 'tp')]
    gather x2 -> x0, local copies, waits for them, and re-layouts: 6.26 us -> none  [the longest x1 3.48 us: local(): normed[source_rows]]
  transfers between devices with their start and end apart: 4 -> 0, of which waited for: 3 -> 0; matrix products, arithmetic and copies ran while one was open for 4% -> 0% of each run, Pallas kernels for 0% -> 0%
where the time goes in v1:
time: 87.9 us; the launch traced here: 87 us
  Pallas kernels  80 us (91%)
  other arithmetic  3.6 us (4%)
  local copies, waits for them, and re-layouts  3.46 us (4%)
    pallas_call x1, Pallas kernels, fused(): pl.pallas_call(functools.partial(fused_kernel, n_chips, capacity), out_sh...  80 us
    unnamed x1, local copies, waits for them, and re-layouts  1.87 us

profile of v1, /device:TPU:0, one launch (start us, length us, event | category | flops | bytes accessed | tf_op | source)
XLA Modules:
  0.0 87.0 jit_solution(3955387450302778442)
XLA Ops:
  0.0 0.8 pad_dynamic-slice_fusion
  0.8 0.1 compare_convert_fusion
  0.8 0.8 compare_select_fusion.3
  1.6 0.8 compare_select_fusion.4
  2.4 0.7 fusion
  3.1 1.3 %broadcast_in_dim.7 = f32[4096]{0:T(1024)} convert(bf16[4096]{0:T(1024)(128)(2,1)} %param.20) | non-fusion elementwise | flops 4096 | bytes 24576 | tf_op jit(solution)/shard_map/broadcast_in_dim | solution.py:492
  4.4 0.8 copy.26.cols_ref
  5.2 80.0 %shard_map.127 = bf16[256,1024]{1,0:T(8,128)(2,1)} custom-call(bf16[256,256]{1,0:T(8,128)(2,1)} %b_ref.1, bf16[256,256]{1,0:T(8,128)(2,1)} %c_ref.1, bf16[256,256]{1,0:T(8,128)(2,1)} %h_ref.1, f32[256,5]{1,0:T(8,128)} %copy.26.cols_ref, bf16[3,1024]{1,0:T(4,128)(2,1)} %taps_ref.1, bf16[256,1024]{1,0:T(8,128)(2,1)} %resid_ref.1, f32[1,4096]{1,0:T(1,128)} %bitcast.3, ...), custom_call_target="tpu_custom_call" | custom-call | tf_op jit(solution)/shard_map/pallas_call | solution.py:497
  85.2 1.9 %copy.28 = bf16[256,1024]{1,0:T(8,128)(2,1)} copy(bf16[256,1024]{1,0:T(8,128)(2,1)} %shard_map.127) | data formatting | bytes 1048576
  (1 shorter events, 0.0 us)

commit v2 on v1

--- a/solution.py
+++ b/solution.py
@@ -9,6 +9,11 @@
 
 TOP_K = 2
 GROUPS = 4
+PLAN = (
+    "S1 F0 S2 F1 S3 D0 E0 F2 D1 E1 X1 F3 D2 E2 X2 R1 D3 E3 X3 "
+    "R2 W1 C1 R3 X0 W2 W3 C2 C3 R0 W0 C0"
+)
+FINAL = (1, 0, 2, 3)
 MESH = pl.DeviceIdType.MESH
 
 
@@ -136,15 +141,19 @@
     b_ref,
     c_ref,
     h_ref,
-    cols_ref,
+    docs_ref,
+    pick_ref,
+    weight_ref,
     taps_ref,
-    resid_ref,
     gain_ref,
+    resid_hbm,
     ow_hbm,
     wg_hbm,
     wu_hbm,
     wd_hbm,
     out_ref,
+    resid,
+    gain,
     ow,
     wg,
     wu,
@@ -170,8 +179,8 @@
     recv_sems,
 ):
     tok_rows, chans = h_ref.shape
-    width = resid_ref.shape[1]
-    full = gain_ref.shape[1]
+    width = resid.shape[1]
+    full = gain_ref.shape[0]
     hid_cols = wg.shape[1]
     sp = lax.axis_index("sp")
     tp = lax.axis_index("tp")
@@ -187,7 +196,7 @@
     dev_z = [(flipped(chip, k) * 2 + core, tp) for k in ks]
 
     loads = []
-    for i, (s, d) in enumerate(((ow_hbm, ow), (wg_hbm.at[0], wg), (wu_hbm.at[0], wu), (wd_hbm.at[0], wd))):
+    for i, (s, d) in enumerate(((ow_hbm, ow), (resid_hbm, resid), (wg_hbm.at[0], wg), (wu_hbm.at[0], wu), (wd_hbm.at[0], wd))):
         cp = pltpu.make_async_copy(s, d, local_sems.at[i])
         cp.start()
         loads.append(cp)
@@ -233,49 +242,66 @@
     def _():
         edge.start()
 
-    lane = lax.broadcasted_iota(jnp.int32, (tok_rows, 128), 1)
-    lane_f = lane.astype(jnp.float32)
-    group = cols_ref[:, 2:3]
-    onehot = (group == lane_f).astype(jnp.float32)
-    earlier = (
-        lax.broadcasted_iota(jnp.int32, (tok_rows, tok_rows), 1)
-        < lax.broadcasted_iota(jnp.int32, (tok_rows, tok_rows), 0)
-    ).astype(jnp.float32).astype(jnp.bfloat16)
-    before = jnp.dot(earlier, onehot.astype(jnp.bfloat16), preferred_element_type=jnp.float32)
-    slot = jnp.sum(before * onehot, axis=1, keepdims=True)
-    for k in ks:
-        here = flipped(chip, k).astype(jnp.float32)
-        hit = jnp.where((group == here) & (slot == lane_f) & (lane < capacity), 1.0, 0.0)
-        pt[k] = hit.astype(jnp.bfloat16)
-    parts = jnp.zeros((tok_rows, 128), jnp.float32)
-    for j in range(2):
-        w = cols_ref[:, 3 + j : 4 + j]
-        for i in range(3):
-            piece = w.astype(jnp.bfloat16).astype(jnp.float32)
-            parts = jnp.where(lane == 3 * j + i, piece, parts)
-            w = w - piece
-    parts = parts.astype(jnp.bfloat16)
-    for k in ks:
-        got = lax.dot_general(
-            pt[k], parts, (((0,), (0,)), ((), ())), preferred_element_type=jnp.float32
-        )
-        wts_out[k] = got[:capacity].astype(jnp.bfloat16)
-    wts[0] = wts_out[0]
-
-    @pl.when(sp > 0)
-    def _():
-        edge.wait_recv()
-
-    @pl.when(sp == 0)
-    def _():
-        ext[0:8, :] = jnp.zeros((8, chans), jnp.float32)
+    row_lane = lax.broadcasted_iota(jnp.int32, (1, tok_rows), 1)
+    own_docs = docs_ref[:, cols(sp, tok_rows)].astype(jnp.float32)
+    last_docs = docs_ref[
+        :, pl.ds(pl.multiple_of(jnp.maximum(sp * tok_rows - 128, 0), 128), 128)
+    ].astype(jnp.float32)
+    one_back = jnp.where(row_lane == 0, last_docs[:, 127:], pltpu.roll(own_docs, 1, 1))
+    two_back = jnp.where(
+        row_lane == 0,
+        last_docs[:, 126:127],
+        jnp.where(row_lane == 1, last_docs[:, 127:], pltpu.roll(own_docs, 2, 1)),
+    )
+    position = row_lane + sp * tok_rows
+    picks = pick_ref[...]
+    odd = picks[0:1] % 2 == 1
+    weight = weight_ref[...]
+    facts = jnp.concatenate(
+        [
+            jnp.where((one_back == own_docs) & (position >= 1), 1.0, 0.0),
+            jnp.where((two_back == own_docs) & (position >= 2), 1.0, 0.0),
+            (picks[0:1] // 2).astype(jnp.float32),
+            jnp.where(odd, weight[1:2], weight[0:1]),
+            jnp.where(odd, weight[0:1], weight[1:2]),
+            jnp.zeros((3, tok_rows), jnp.float32),
+        ],
+        axis=0,
+    ).T
+    def make_slots():
+        lane = lax.broadcasted_iota(jnp.int32, (tok_rows, 128), 1)
+        lane_f = lane.astype(jnp.float32)
+        group = facts[:, 2:3]
+        onehot = (group == lane_f).astype(jnp.float32)
+        earlier = (
+            lax.broadcasted_iota(jnp.int32, (tok_rows, tok_rows), 1)
+            < lax.broadcasted_iota(jnp.int32, (tok_rows, tok_rows), 0)
+        ).astype(jnp.float32).astype(jnp.bfloat16)
+        before = jnp.dot(earlier, onehot.astype(jnp.bfloat16), preferred_element_type=jnp.float32)
+        slot = jnp.sum(before * onehot, axis=1, keepdims=True)
+        for k in ks:
+            here = flipped(chip, k).astype(jnp.float32)
+            hit = jnp.where((group == here) & (slot == lane_f) & (lane < capacity), 1.0, 0.0)
+            pt[k] = hit.astype(jnp.bfloat16)
+        parts = jnp.zeros((tok_rows, 128), jnp.float32)
+        for j in range(2):
+            w = facts[:, 3 + j : 4 + j]
+            for i in range(3):
+                piece = w.astype(jnp.bfloat16).astype(jnp.float32)
+                parts = jnp.where(lane == 3 * j + i, piece, parts)
+                w = w - piece
+        parts = parts.astype(jnp.bfloat16)
+        for k in ks:
+            got = lax.dot_general(
+                pt[k], parts, (((0,), (0,)), ((), ())), preferred_element_type=jnp.float32
+            )
+            wts_out[k] = got[:capacity].astype(jnp.bfloat16)
+        wts[0] = wts_out[0]
+
+    gain[...] = gain_ref[...].astype(jnp.float32)[None, :]
 
     taps = taps_ref[:, cols(tp, chans)].astype(jnp.float32)
-    conv = taps[0:1, :] * ext[8 : 8 + tok_rows, :]
-    for lag in (1, 2):
-        conv = conv + taps[lag : lag + 1, :] * ext[8 - lag : 8 - lag + tok_rows, :] * cols_ref[:, lag - 1 : lag]
-    conv = (b_ref[...].astype(jnp.float32) * conv).astype(jnp.bfloat16)
-    cv[:, cols(tp, chans)] = conv
+    half_rows = tok_rows // 2
 
     def spread(buf, size, own_sends):
         mine = buf.at[:, cols(tp, size)]
@@ -291,21 +317,53 @@
         part = buf.at[:, cols(tp_x * 2 + 1, half)]
         sends.append(go(part, part, dev_y))
 
-    conv_sends = []
-    spread(cv, chans, conv_sends)
-
-    def proj(index):
+    def convolve(h):
+        at = h * half_rows
+        conv = taps[0:1, :] * ext[8 + at : 8 + at + half_rows, :]
+        for lag in (1, 2):
+            conv = (
+                conv
+                + taps[lag : lag + 1, :]
+                * ext[8 + at - lag : 8 + at - lag + half_rows, :]
+                * facts[at : at + half_rows, lag - 1 : lag]
+            )
+        gate = b_ref[at : at + half_rows, :].astype(jnp.float32)
+        cv[h, :, cols(tp, chans)] = (gate * conv).astype(jnp.bfloat16)
+        spread(cv.at[h], chans, conv_sends[h])
+
+    conv_sends = [[], []]
+    convolve(1)
+
+    @pl.when(sp > 0)
+    def _():
+        edge.wait_recv()
+
+    @pl.when(sp == 0)
+    def _():
+        ext[0:8, :] = jnp.zeros((8, chans), jnp.float32)
+
+    convolve(0)
+
+    def proj(h, index):
         rows_ = pl.ds(pl.multiple_of(index * chans, 128), chans)
-        return jnp.dot(cv[:, cols(index, chans)], ow[rows_, :], preferred_element_type=jnp.float32)
-
+        return jnp.dot(cv[h, :, cols(index, chans)], ow[rows_, :], preferred_element_type=jnp.float32)
+
+    make_slots()
     loads[0].wait()
-    acc[...] = resid_ref[...].astype(jnp.float32) + proj(tp)
-    relay(cv, chans, conv_sends)
-    acc[...] += proj(tp_x)
-    acc[...] += proj(tp_y)
-    conv_sends[2].wait_recv()
-    conv_sends[3].wait_recv()
-    stream[...] = (acc[...] + proj(tp_d)).astype(jnp.bfloat16)
+    loads[1].wait()
+    half_at = [pl.ds(h * half_rows, half_rows) for h in range(2)]
+    relay(cv.at[1], chans, conv_sends[1])
+    for h in (1, 0):
+        acc[half_at[h], :] = resid[half_at[h], :].astype(jnp.float32) + proj(h, tp)
+    acc[half_at[1], :] += proj(1, tp_x)
+    acc[half_at[1], :] += proj(1, tp_y)
+    relay(cv.at[0], chans, conv_sends[0])
+    acc[half_at[0], :] += proj(0, tp_x)
+    acc[half_at[0], :] += proj(0, tp_y)
+    for h in (1, 0):
+        conv_sends[h][2].wait_recv()
+        conv_sends[h][3].wait_recv()
+        stream[half_at[h], :] = (acc[half_at[h], :] + proj(h, tp_d)).astype(jnp.bfloat16)
 
     z_rows, z_wts = [None] * n_chips, [None] * n_chips
     mine = cols(tp, width)
@@ -359,13 +417,13 @@
                 x = rows[k, p, at, :].astype(jnp.float32)
                 ms = jnp.sum(x * x, axis=1, keepdims=True) / full
                 inv = lax.rsqrt(ms + NORM_EPS)
-                y = (x * inv * gain_ref[...]).astype(jnp.bfloat16)
+                y = (x * inv * gain[...]).astype(jnp.bfloat16)
                 normed[pl.ds(pl.multiple_of(p * capacity + r * 16, 16), 16), :] = y
                 return carry
             lax.fori_loop(0, capacity // 16, norm, 0)
         if k == 0:
-            loads[1].wait()
             loads[2].wait()
+            loads[3].wait()
 
         def tile(n, carry):
             at = pl.ds(pl.multiple_of(n * 256, 256), 256)
@@ -377,19 +435,22 @@
             return carry
 
         lax.fori_loop(0, hid_cols // 256, tile, 0)
+
+    def hid_send(k):
         spread(hid.at[k], hid_cols, hid_sends[k])
 
     def hid_forward(k):
         relay(hid.at[k], hid_cols, hid_sends[k])
 
     e_sends = [None] * n_chips
+    late_loads = [loads[4]]
     z_back = [None] * n_chips
 
     def down(k):
         hid_sends[k][2].wait_recv()
         hid_sends[k][3].wait_recv()
-        if k == 0:
-            loads[3].wait()
+        while late_loads:
+            late_loads.pop().wait()
 
         def tile(n, carry):
             at = pl.ds(pl.multiple_of(n * 256, 256), 256)
@@ -422,22 +483,15 @@
     for k in ks:
         back[k, capacity:, :] = jnp.zeros((128 - capacity, width), jnp.bfloat16)
 
-    last = n_chips - 1
-    plan = sorted(
-        [(3 * k, 0, stage, k) for k in ks]
-        + [(3 * k + 4, 1, forward, k) for k in ks]
-        + [(3 * k + 7, 2, finish, k) for k in ks]
-        + [(3 * k + 9, 3, expand, k) for k in ks]
-        + [(3 * k + 13, 4, hid_forward, k) for k in ks]
-        + [(3 * k + 16, 5, down, k) for k in ks]
-        + [(3 * k + 18, 6, combine, k) for k in ks],
-        key=lambda item: item[:2],
-    )
-    for _, _, step, k in plan:
-        step(k)
+    steps = {
+        "S": stage, "F": forward, "D": finish, "E": expand, "X": hid_send,
+        "R": hid_forward, "W": down, "C": combine,
+    }
+    for step in PLAN.split():
+        steps[step[0]](int(step[1:]))
 
     acc[...] = stream[...].astype(jnp.float32)
-    for k in ks:
+    for k in FINAL:
         if k > 0:
             z_back[k].wait_recv()
         acc[...] += jnp.dot(pt[k], back[k], preferred_element_type=jnp.float32)
@@ -474,38 +528,24 @@
     n_sp = lax.axis_size("sp")
     n_chips = n_sp // 2
     capacity = 5 * tok_rows // (2 * n_sp)
-    first_pos = lax.axis_index("sp") * tok_rows
-    padded_docs = jnp.concatenate([jnp.full((2,), -1, jnp.int32), docs], axis=0)
-    near = lax.dynamic_slice_in_dim(padded_docs, first_pos, tok_rows + 2)
-    own = near[2:]
-    even = expert_pick[:, 0] % 2 == 0
-    side = jnp.stack(
-        [
-            (near[1:-1] == own).astype(jnp.float32),
-            (near[:-2] == own).astype(jnp.float32),
-            (expert_pick[:, 0] // 2).astype(jnp.float32),
-            jnp.where(even, route_weight[:, 0], route_weight[:, 1]),
-            jnp.where(even, route_weight[:, 1], route_weight[:, 0]),
-        ],
-        axis=1,
-    )
-    gain = norm_gain.astype(jnp.float32)[None, :]
-    n_copies = 5 + 2 * (n_chips - 1) + 14 * n_chips + n_chips - 1
+    n_copies = 9 + 2 * (n_chips - 1) + 14 * n_chips + n_chips - 1
     vmem = pl.BlockSpec(memory_space=pltpu.VMEM)
     hbm = pl.BlockSpec(memory_space=pl.ANY)
     bf16 = jnp.bfloat16
     return pl.pallas_call(
         functools.partial(fused_kernel, n_chips, capacity),
         out_shape=jax.ShapeDtypeStruct((tok_rows, width), bf16),
-        in_specs=[vmem] * 7 + [hbm] * 4,
+        in_specs=[vmem] * 8 + [hbm] * 5,
         out_specs=vmem,
         scratch_shapes=[
+            pltpu.VMEM(residual_in.shape, bf16),
+            pltpu.VMEM((1, full), jnp.float32),
             pltpu.VMEM(out_weight.shape, bf16),
             pltpu.VMEM(w_gate.shape[1:], bf16),
             pltpu.VMEM(w_up.shape[1:], bf16),
             pltpu.VMEM(w_down.shape[1:], bf16),
             pltpu.VMEM((tok_rows + 8, chans), jnp.float32),
-            pltpu.VMEM((tok_rows, out_weight.shape[0]), bf16),
+            pltpu.VMEM((2, tok_rows // 2, out_weight.shape[0]), bf16),
             pltpu.VMEM((tok_rows, width), bf16),
             pltpu.VMEM((tok_rows, width), jnp.float32),
             pltpu.VMEM((n_chips, tok_rows, 128), bf16),
@@ -520,14 +560,28 @@
             pltpu.VMEM((n_chips, capacity, width), bf16),
             pltpu.VMEM((n_chips, capacity, width), bf16),
             pltpu.VMEM((n_chips, 128, width), bf16),
-            pltpu.SemaphoreType.DMA((4,)),
+            pltpu.SemaphoreType.DMA((5,)),
             pltpu.SemaphoreType.DMA((n_copies,)),
             pltpu.SemaphoreType.DMA((n_copies,)),
         ],
         compiler_params=pltpu.CompilerParams(
             collective_id=0, has_side_effects=True, vmem_limit_bytes=56 * 1024 * 1024
         ),
-    )(b_gate, c_gate, h_in, side, conv_taps, residual_in, gain, out_weight, w_gate, w_up, w_down)
+    )(
+        b_gate,
+        c_gate,
+        h_in,
+        docs[None, :],
+        expert_pick.T,
+        route_weight.T,
+        conv_taps,
+        norm_gain,
+        residual_in,
+        out_weight,
+        w_gate,
+        w_up,
+        w_down,
+    )
 
 
 def pairs_fit(mesh):

time: 87.9 us -> 80.2 us (0.912)
  other arithmetic: 3.6 us -> 0 us
  Pallas kernels: 80 us -> 78.2 us
  local copies, waits for them, and re-layouts: 3.46 us -> 1.87 us
    pallas_call x1, Pallas kernels: 80 us -> 78.2 us  [fused(): pl.pallas_call(functools.partial(fused_kernel, n_chips, capacity), out_sh...]
    select_n x2 -> x0, other arithmetic: 1.53 us -> none  [the longest x1 0.77 us: fused(): jnp.where(even, route_weight[:, 1], route_weight[:, 0])]
    broadcast_in_dim x1 -> x0, other arithmetic: 1.3 us -> none  [fused(): gain = norm_gain.astype(jnp.float32)[None, :]]
where the time goes in v2:
time: 80.2 us; the launch traced here: 80 us
  Pallas kernels  78.2 us (98%)
  local copies, waits for them, and re-layouts  1.87 us (2%)
    pallas_call x1, Pallas kernels, fused(): pl.pallas_call(functools.partial(fused_kernel, n_chips, capacity), out_sh...  78.2 us
    unnamed x1, local copies, waits for them, and re-layouts  1.87 us

profile of v2, /device:TPU:0, one launch (start us, length us, event | category | flops | bytes accessed | tf_op | source)
XLA Modules:
  0.0 80.0 jit_solution(18162290796567263239)
XLA Ops:
  0.0 78.2 %shard_map.127 = bf16[256,1024]{1,0:T(8,128)(2,1)} custom-call(bf16[256,256]{1,0:T(8,128)(2,1)} %b_ref.1, bf16[256,256]{1,0:T(8,128)(2,1)} %c_ref.1, bf16[256,256]{1,0:T(8,128)(2,1)} %h_ref.1, s32[1,2048]{1,0:T(1,128)} %bitcast.3, s32[2,256]{1,0:T(2,128)} %bitcast.4, f32[2,256]{1,0:T(2,128)} %bitcast.5, bf16[3,1024]{1,0:T(4,128)(2,1)} %taps_ref.1, ...), custom_call_target="tpu_custom_call" | custom-call | tf_op jit(solution)/shard_map/pallas_call | solution.py:535
  78.2 1.9 %copy.15 = bf16[256,1024]{1,0:T(8,128)(2,1)} copy(bf16[256,1024]{1,0:T(8,128)(2,1)} %shard_map.127) | data formatting | bytes 1048576
